TPU v7x, 32 devices: a whole 2x2x4 slice. The times are simulated.
32 devices in a mesh: ep: 4 (over y, x), tp: 8 (over z, core).
Axes of the slice: x: 2, y: 2, z: 4, core: 2. Of those that a mesh axis runs over, the one named last changes fastest.
Arguments:
- queries: bfloat16 [16, 64, 2, 512], P('tp', None, None, 'ep'), may hold values from -24 to 24
- key_vectors: bfloat16 [16, 64, 2, 512], P('tp', None, None, 'ep'), may hold values from -24 to 24
- value_vectors: bfloat16 [16, 64, 2, 512], P('tp', None, None, 'ep'), may hold values from -6 to 6
- mixer_weight: bfloat16 [1024, 2048], replicated, may hold values from -0.375 to 0.375
- expert_rows: bfloat16 [512, 2048], P('ep'), may hold values from -6 to 6
- norm_gain: float32 [2048], replicated, may hold values from 0.1 to 1.9
- route_ids: int32 [512, 2], P('ep'), may hold values from 0 to 7, all different within a row; in each aligned block of 128 rows (0 to 127, 128 to 255, ...) at most 64 rows name the same one
- route_logits: float32 [512, 2], P('ep'), may hold values from -4 to 4
- gate_weight: bfloat16 [8, 2048, 4096], P('ep', None, 'tp'), may hold values from -0.39648438 to 0.39648438
- up_weight: bfloat16 [8, 2048, 4096], P('ep', None, 'tp'), may hold values from -0.39648438 to 0.39648438
- down_weight: bfloat16 [8, 4096, 2048], P('ep', 'tp'), may hold values from -0.028076172 to 0.028076172
Outputs:
- mixer_out: bfloat16 [2, 512, 2048], P(None, ('ep', 'tp'))
- routed_out: bfloat16 [2048, 512], P('tp', 'ep')
Inputs may be any that keep to these rules, and one draw needn't show every extreme that they name: `route_ids`: each row names 2 different experts. Among the 128 rows of one index of ep no expert is named more than 64 times, a bound that some expert reaches in such a block.
All inputs are finite; a program needn't handle non-finite values.
Results may differ from a plain program's by a relative error of at most 0.018.
Values may be sent and summed in bfloat16 or wider, within the bound.
No kernel may reach another device: no remote copies, remote signals or barrier semaphores. Data moves between devices by JAX's collectives and lax.ppermute only.
A program may use at most 64 MiB of HBM per device.

v0:
```python
import jax
import jax.numpy as jnp
from jax import lax
from jax.sharding import PartitionSpec as P

limit_value = 7.0
alpha_value = 1.702
norm_eps = 1e-06


def activate(gate_pre, up_pre):
    gate_clamped = jnp.minimum(gate_pre, limit_value)
    up_clamped = jnp.clip(up_pre, -limit_value, limit_value)
    return ((up_clamped + 1.0) * gate_clamped * jax.nn.sigmoid(alpha_value * gate_clamped)).astype(
        jnp.bfloat16
    )


def block_terms(query_rows, key_block, value_block, block_index, own_index):
    seg_len = query_rows.shape[3]
    score_scale = query_rows.shape[1] ** (-0.5)
    scores = (
        jnp.einsum("hdsq,hdsk->hsqk", query_rows, key_block, preferred_element_type=jnp.float32)
        * score_scale
    )
    query_pos = lax.broadcasted_iota(jnp.int32, (seg_len, seg_len), 0)
    lookup_slot = lax.broadcasted_iota(jnp.int32, (seg_len, seg_len), 1)
    usable = jnp.logical_or(block_index < own_index, lookup_slot < query_pos)
    log_keep = jnp.where(usable, jax.nn.log_sigmoid(-scores), 0.0)
    within = lax.cumsum(log_keep, axis=3, reverse=True) - log_keep
    weight = jnp.where(usable, jnp.exp(jax.nn.log_sigmoid(scores) + within), 0.0).astype(
        jnp.bfloat16
    )
    block_out = jnp.einsum(
        "hsqk,hdsk->hdsq", weight, value_block, preferred_element_type=jnp.float32
    )
    return (block_out, jnp.sum(log_keep, axis=3))


def attend(query_rows, key_vectors, value_vectors):
    head_count, head_dim, seq_count, seg_len = query_rows.shape
    blocks = lax.axis_size("ep")
    own_index = lax.axis_index("ep")
    first_outs = jnp.zeros((blocks, head_count, head_dim, seq_count, seg_len), jnp.float32)
    first_totals = jnp.zeros((blocks, head_count, seq_count, seg_len), jnp.float32)
    key_piece = lax.all_gather(key_vectors, "ep", axis=3, tiled=True)
    value_piece = lax.all_gather(value_vectors, "ep", axis=3, tiled=True)
    shard_count = key_piece.shape[3] // seg_len

    def one_block(offset, inner_state):
        block_outs, block_totals = inner_state
        key_block = lax.dynamic_slice_in_dim(key_piece, offset * seg_len, seg_len, 3)
        value_block = lax.dynamic_slice_in_dim(value_piece, offset * seg_len, seg_len, 3)

        def compute(unused):
            return block_terms(query_rows, key_block, value_block, offset, own_index)

        def skip_block(unused):
            return (
                jnp.zeros((head_count, head_dim, seq_count, seg_len), jnp.float32),
                jnp.zeros((head_count, seq_count, seg_len), jnp.float32),
            )

        block_out, block_total = lax.cond(offset <= own_index, compute, skip_block, 0)
        block_outs = lax.dynamic_update_index_in_dim(block_outs, block_out, offset, 0)
        block_totals = lax.dynamic_update_index_in_dim(block_totals, block_total, offset, 0)
        return (block_outs, block_totals)

    block_outs, block_totals = lax.fori_loop(0, shard_count, one_block, (first_outs, first_totals))
    later_sums = lax.cumsum(block_totals, axis=0, reverse=True) - block_totals
    return jnp.sum(jnp.exp(later_sums)[:, :, None] * block_outs, axis=0).astype(jnp.bfloat16)


def mix_heads(attended, mixer_weight):
    head_count, head_dim, seq_count, seg_len = attended.shape
    flat_heads = attended.reshape(head_count * head_dim, seq_count, seg_len)
    return jnp.einsum(
        "csr,cm->srm",
        lax.all_to_all(flat_heads, "tp", split_axis=2, concat_axis=0, tiled=True),
        mixer_weight,
        preferred_element_type=jnp.float32,
    ).astype(jnp.bfloat16)


def expert_block(send_rows, gate_portion, up_part, down_part):
    groups = lax.axis_size("ep")
    local_experts = gate_portion.shape[0]
    cap_rows = send_rows.shape[1]
    model_width = send_rows.shape[2]
    received = lax.all_to_all(send_rows, "ep", split_axis=0, concat_axis=0, tiled=True)
    bucketed = received.reshape(groups, local_experts, cap_rows, model_width)
    gate_pre = jnp.einsum(
        "sjcd,jdf->sjcf", bucketed, gate_portion, preferred_element_type=jnp.float32
    )
    up_pre = jnp.einsum("sjcd,jdf->sjcf", bucketed, up_part, preferred_element_type=jnp.float32)
    hidden = activate(gate_pre, up_pre)
    slot_total = groups * local_experts * cap_rows
    term_rows = jnp.einsum("sjcf,jfd->dsjc", hidden, down_part, preferred_element_type=jnp.float32)
    summed = lax.psum_scatter(
        term_rows.reshape(
            model_width // lax.axis_size("tp") * lax.axis_size("tp"), slot_total
        ).astype(jnp.bfloat16),
        "tp",
        scatter_dimension=0,
        tiled=True,
    ).astype(jnp.float32)
    return lax.all_to_all(
        summed.astype(jnp.bfloat16), "ep", split_axis=1, concat_axis=1, tiled=True
    ).astype(summed.dtype)


def route_experts(
    expert_rows, norm_gain, route_ids, route_logits, gate_weight, up_weight, down_weight
):
    groups = lax.axis_size("ep")
    local_experts = gate_weight.shape[0]
    expert_count = groups * local_experts
    token_rows, top_count = route_ids.shape
    cap_rows = 2 * token_rows * top_count // expert_count
    values = expert_rows.astype(jnp.float32)
    scaled = values * lax.rsqrt(jnp.mean(values * values, axis=-1, keepdims=True) + norm_eps)
    normed = (scaled * norm_gain).astype(jnp.bfloat16)
    route_weight = jax.nn.softmax(route_logits, axis=-1)
    flat_ids = route_ids.reshape(token_rows * top_count)
    one_hot_matrix = (
        flat_ids[:, None] == jnp.arange(expert_count, dtype=jnp.int32)[None, :]
    ).astype(jnp.int32)
    earlier = jnp.cumsum(one_hot_matrix, axis=0) - one_hot_matrix
    slot_rank = jnp.sum(earlier * one_hot_matrix, axis=1)
    column = flat_ids * cap_rows + slot_rank
    token_index = jnp.arange(token_rows * top_count, dtype=jnp.int32) // top_count
    owner_token = jnp.zeros((expert_count * cap_rows,), jnp.int32).at[column].set(token_index)
    filled = jnp.zeros((expert_count * cap_rows,), jnp.int32).at[column].set(1)
    send_rows = jnp.where(filled[:, None] > 0, normed[owner_token], jnp.zeros((), jnp.bfloat16))
    send_rows = send_rows.reshape(groups, local_experts, cap_rows, normed.shape[1])
    halves = 1
    per_half = local_experts // halves
    part_rows = send_rows.reshape(groups * per_half, cap_rows, normed.shape[1])
    result = expert_block(part_rows, gate_weight, up_weight, down_weight)
    results = result.reshape(result.shape[0], groups, per_half, cap_rows)
    gathered = results.reshape(results.shape[0], expert_count * cap_rows)
    picked = jnp.take(gathered, column, axis=1).reshape(gathered.shape[0], token_rows, top_count)
    combined = jnp.sum(picked * route_weight[None], axis=2)
    return combined.astype(jnp.bfloat16)


def body(
    queries,
    key_vectors,
    value_vectors,
    mixer_weight,
    expert_rows,
    norm_gain,
    route_ids,
    route_logits,
    gate_weight,
    up_weight,
    down_weight,
):
    attended = attend(queries, key_vectors, value_vectors)
    mixer_out = mix_heads(attended, mixer_weight)
    routed_out = route_experts(
        expert_rows, norm_gain, route_ids, route_logits, gate_weight, up_weight, down_weight
    )
    return (mixer_out, routed_out)


def solution(mesh):
    in_specs = (
        P("tp", None, None, "ep"),
        P("tp", None, None, "ep"),
        P("tp", None, None, "ep"),
        P(),
        P("ep", None),
        P(),
        P("ep", None),
        P("ep", None),
        P("ep", None, "tp"),
        P("ep", None, "tp"),
        P("ep", "tp", None),
    )
    out_specs = (P(None, ("ep", "tp"), None), P("tp", "ep"))
    return jax.shard_map(body, mesh=mesh, in_specs=in_specs, out_specs=out_specs, check_vma=False)
```

profile of v0, /device:TPU:0, one launch (start us, length us, event | category | flops | bytes accessed | tf_op | source)
XLA Modules:
  0.0 130.4 jit_solution(11275441368211532716)
XLA Ops:
  7.2 0.8 copy.67
  10.2 1.4 %scatter_custom_fusion.1 = s32[512]{0:T(512)S(1)} fusion(s32[256]{0:T(256)S(1)} %bitcast.93, s32[256]{0:T(256)S(1)} %and_select_fusion, s32[]{:T(128)} %copy.121), kind=kCustom, calls=%fused_computation.82 | custom fusion | bytes 2052 | tf_op jit(solution)/shard_map/scatter | solution.py:132
  11.6 1.2 fusion.73
  12.8 1.4 %scatter_custom_fusion = s32[512]{0:T(512)S(1)} fusion(s32[256]{0:T(256)S(1)} %bitcast.94, s32[256]{0:T(256)S(1)} %broadcast.130, s32[]{:T(128)} %copy.121), kind=kCustom, calls=%fused_computation.85 | custom fusion | bytes 2052 | tf_op jit(solution)/shard_map/scatter | solution.py:133
  14.3 1.2 fusion.75
  15.6 2.5 %gather_fusion = bf16[512,2048]{1,0:T(8,128)(2,1)S(1)} fusion(bf16[128,2048]{1,0:T(8,128)(2,1)S(1)} %fusion.75, s32[1024]{0:T(1024)S(1)} %pad_clamp_fusion.1), kind=kCustom, calls=%fused_computation | custom fusion | bytes 4196352 | tf_op jit(solution)/shard_map/gather | solution.py:134
  18.3 30.6 %all_to_all.32 = bf16[8,64,2048]{2,1,0:T(8,128)(2,1)S(1)} all-to-all(bf16[8,64,2048]{2,1,0:T(8,128)(2,1)S(1)} %broadcast_select_fusion), channel_id=1, replica_groups=mesh['ep'=4,'tp'=8] {'ep'}, dimensions={0} | all-to-all | bytes 4194304 | tf_op jit(solution)/shard_map/all_to_all | solution.py:90
  48.9 1.2 fusion.57
  50.2 7.3 %fusion.29 = bf16[2048,4,2,64]{0,3,1,2:T(8,128)(2,1)} fusion(bf16[2,512,2048]{2,1,0:T(8,128)(2,1)} %param.25, f32[2,4,64,512]{3,2,1,0:T(8,128)S(1)} %fusion.57, bf16[2,2048,512]{2,1,0:T(8,128)(2,1)} %param.24, bf16[4,2,64,2048]{3,2,1,0:T(8,128)(2,1)S(1)} %bitcast.86), kind=kOutput, calls=%fused_computation.36 | convolution fusion | flops 2150891520 | bytes 13631488 | tf_op jit(solution)/shard_map/sjcf,jfd->dsjc/dot_general | solution.py:98
  57.4 3.2 %copy.74 = bf16[2048,4,2,64]{0,3,2,1:T(8,128)(2,1)} copy(bf16[2048,4,2,64]{0,3,1,2:T(8,128)(2,1)} %fusion.29) | data formatting | bytes 4194304 | tf_op jit(solution)/shard_map/convert_element_type | solution.py:102
  60.7 0.8 copy-done
  61.6 8.6 %all_gather.6 = bf16[2,64,2,512]{3,1,2,0:T(8,128)(2,1)S(1)} all-gather(bf16[2,64,2,128]{3,1,2,0:T(8,128)(2,1)S(1)} %copy.60), channel_id=1, replica_groups=mesh['ep'=4,'tp'=8] {'ep'}, dimensions={3}, use_global_device_ids=true | all-gather | bytes 327680 | tf_op jit(solution)/shard_map/all_gather | solution.py:46
  70.2 8.9 %all_gather.7 = bf16[2,64,2,512]{3,1,2,0:T(8,128)(2,1)S(1)} all-gather(bf16[2,64,2,128]{3,1,2,0:T(8,128)(2,1)S(1)} %copy.61), channel_id=1, replica_groups=mesh['ep'=4,'tp'=8] {'ep'}, dimensions={3}, use_global_device_ids=true | all-gather | bytes 327680 | tf_op jit(solution)/shard_map/all_gather | solution.py:47
  79.1 5.8 %while.15 = (s32[]{:T(128)}, f32[4,2,64,2,128]{4,2,3,1,0:T(8,128)S(1)}, f32[4,2,2,128]{3,2,1,0:T(2,128)S(1)}, s32[]{:T(128)}, bf16[2,64,2,512]{3,1,2,0:T(8,128)(...) while((s32[]{:T(128)}, ...), condition=%wide.region_5.6_spmd, body=%wide.region_0.5_spmd.sunk | while | flops 27098632 | bytes 2218215 | solution.py:69
  79.1 5.4 %conditional.2 = (f32[1,2,64,2,128]{4,2,3,1,0:T(8,128)S(1)}, f32[1,2,2,128]{3,2,1,0:T(2,128)S(1)}) conditional(s32[]{:T(128)} %convert_element_type.99, () %tuple.66, (s32[]{:T(128)}, s32[]{:T(128)}, bf16[2,64,2,512]{3,1,2,0:T(8,128)(2,1)S(1)}, bf16[2,64,2,128]{3,1,2,0:T(8,128)(2,1)S(1)}, bf16[2,64,2,512]{3,1,2,0:T(8,128)(2,1)S(1)}) %tuple.67), branch_computations={%region_1.0_spmd, %region_2.4_spmd} | conditional | flops 27098628 | bytes 1951828 | solution.py:64
  79.5 4.4 %reduce_window_sum.35 = f32[2,2,128,128]{2,3,1,0:T(8,128)S(1)} reduce-window(f32[2,2,128,128]{2,3,1,0:T(8,128)S(1)} %get-tuple-element.277, f32[]{:T(128)} %constant.130.clone), window={size=1x1x1x128 pad=0_0x0_0x0_0x0_127}, to_apply=%region_3.2 | reduce-window | flops 8323072 | bytes 524292 | tf_op jit(solution)/shard_map/while/body/eval_jaxpr/cond/branch_1_fun/reduce_window_sum | solution.py:30
  84.9 0.8 copy.64
  85.7 4.9 %all-to-all-start = ((bf16[128,2,128]{0,1,2:T(2,128)(2,1)}), bf16[128,2,128]{0,1,2:T(2,128)(2,1)S(1)}, u32[]{:S(2)}, u32[]{:S(2)}) async-start(bf16[128,2,128]{0,1,2:T(2,128)(2,1)} %copy.64), calls=%async_computation | async-start | bytes 131072 | tf_op jit(solution)/shard_map/all_to_all | solution.py:79
  91.1 5.4 %all-to-all-done = bf16[128,2,128]{0,1,2:T(2,128)(2,1)S(1)} async-done(((bf16[128,2,128]{0,1,2:T(2,128)(2,1)}), bf16[128,2,128]{0,1,2:T(2,128)(2,1)S(1)}, u32[]{:S(2)}, u32[]{:S(2)}) %all-to-all-start) | async-done | bytes 65568 | tf_op jit(solution)/shard_map/all_to_all | solution.py:79
  96.8 18.6 %all-to-all-start.2 = ((bf16[256,4,128]{0,2,1:T(8,128)(2,1)}), bf16[256,4,128]{0,2,1:T(8,128)(2,1)S(1)}, u32[]{:S(2)}, u32[]{:S(2)}) async-start(bf16[256,4,128]{0,2,1:T(8,128)(2,1)} %bitcast.89), calls=%async_computation.3 | async-start | bytes 524288 | tf_op jit(solution)/shard_map/all_to_all | solution.py:107
  115.3 3.7 %fusion.32 = bf16[2,16,2048]{2,1,0:T(8,128)(2,1)} fusion(bf16[1024,2048]{1,0:T(8,128)(2,1)} %param.18, bf16[2,8,2,8,128]{4,3,2,1,0:T(8,128)(2,1)S(1)} %bitcast.88), kind=kOutput, calls=%fused_computation.37 | convolution fusion | flops 134283264 | bytes 4390912 | tf_op jit(solution)/shard_map/csr,cm->srm/dot_general | solution.py:77
  119.0 1.7 %all-to-all-done.2 = bf16[256,4,128]{0,2,1:T(8,128)(2,1)S(1)} async-done(((bf16[256,4,128]{0,2,1:T(8,128)(2,1)}), bf16[256,4,128]{0,2,1:T(8,128)(2,1)S(1)}, u32[]{:S(2)}, u32[]{:S(2)}) %all-to-all-start.2) | async-done | bytes 262176 | tf_op jit(solution)/shard_map/all_to_all | solution.py:107
  120.8 1.0 gather_fusion.1
  121.9 0.9 multiply_reduce_fusion.1
  (75 shorter events, 5.6 us)
Async XLA Ops:
  7.2 89.6 %reduce-scatter.2.cloned.1.call-start = ((), (), s32[]{:S(2)}) async-start(), calls=%async_computation.4 | async-start | bytes 2359296 | tf_op jit(solution)/shard_map/reduce_scatter | solution.py:99
  18.3 30.6 %copy-start.5 = (bf16[2,2048,512]{2,1,0:T(8,128)(2,1)S(1)}, bf16[2,2048,512]{2,1,0:T(8,128)(2,1)}, u32[]{:S(2)}) copy-start(bf16[2,2048,512]{2,1,0:T(8,128)(2,1)} %param.23) | copy-start | bytes 12582916
  60.6 0.8 copy-start
  60.6 0.9 copy-start.1
  60.6 0.9 copy-start.2
  79.0 11.7 %copy-start.4 = (f32[128,2]{0,1:T(2,128)S(1)}, f32[128,2]{0,1:T(2,128)}, u32[]{:S(2)}) copy-start(f32[128,2]{0,1:T(2,128)} %param.22) | copy-start | bytes 3076
  79.1 11.8 %copy-start.3 = (s32[128,2]{0,1:T(2,128)S(1)}, s32[128,2]{0,1:T(2,128)}, u32[]{:S(2)}) copy-start(s32[128,2]{0,1:T(2,128)} %param.21) | copy-start | bytes 3076
  85.7 10.8 %all-to-all-start = ((bf16[128,2,128]{0,1,2:T(2,128)(2,1)}), bf16[128,2,128]{0,1,2:T(2,128)(2,1)S(1)}, u32[]{:S(2)}, u32[]{:S(2)}) async-start(bf16[128,2,128]{0,1,2:T(2,128)(2,1)} %copy.64), calls=%async_computation | async-start | bytes 131072 | tf_op jit(solution)/shard_map/all_to_all | solution.py:79
  96.8 23.9 %all-to-all-start.2 = ((bf16[256,4,128]{0,2,1:T(8,128)(2,1)}), bf16[256,4,128]{0,2,1:T(8,128)(2,1)S(1)}, u32[]{:S(2)}, u32[]{:S(2)}) async-start(bf16[256,4,128]{0,2,1:T(8,128)(2,1)} %bitcast.89), calls=%async_computation.3 | async-start | bytes 524288 | tf_op jit(solution)/shard_map/all_to_all | solution.py:107
Sparse Core Ops, SparseCore 0:
  60.8 35.9 reduce-scatter.1
where the time goes:
time: 131 us; the launch traced here: 130 us
  blocking collectives  48.1 us (37%)
  starting transfers between devices  23.5 us (18%)
  between operations  14.3 us (11%)
  local copies, waits for them, and re-layouts  14.2 us (11%)
  matrix products  13.1 us (10%)
  other arithmetic  9.63 us (7%)
  waiting for transfers between devices  7.31 us (6%)
    all_to_all x1, blocking collectives, expert_block(): lax.all_to_all(send_rows, 'ep', split_axis=0, concat_axis=0, tiled=True)  30.6 us
    all_to_all x1, starting transfers between devices, expert_block(): lax.all_to_all(summed.astype(jnp.bfloat16), 'ep', split_axis=1, concat_ax...  18.6 us
    all_gather x1, blocking collectives, attend(): value_piece = lax.all_gather(value_vectors, 'ep', axis=3, tiled=True)  8.89 us
    all_gather x1, blocking collectives, attend(): key_piece = lax.all_gather(key_vectors, 'ep', axis=3, tiled=True)  8.6 us
    dot_general x1, matrix products, expert_block(): jnp.einsum('sjcf,jfd->dsjc', hidden, down_part, preferred_element_type=jn...  7.28 us
    all_to_all x1, waiting for transfers between devices, mix_heads(): lax.all_to_all(flat_heads, 'tp', split_axis=2, concat_axis=0, tiled=True)  5.35 us
    all_to_all x1, starting transfers between devices, mix_heads(): lax.all_to_all(flat_heads, 'tp', split_axis=2, concat_axis=0, tiled=True)  4.88 us
    another operation x1, other arithmetic, block_terms(): within = lax.cumsum(log_keep, axis=3, reverse=True) - log_keep  4.43 us
  transfers between devices with their start and end apart: 3, of which 3 were waited for; matrix products, arithmetic and copies ran while one was open for 8% of the time, Pallas kernels for 0%

commit v1 on v0

--- a/solution.py
+++ b/solution.py
@@ -6,6 +6,13 @@
 limit_value = 7.0
 alpha_value = 1.702
 norm_eps = 1e-06
+
+
+def trade_parts(x, axis, split, join):
+    peers = lax.axis_size(axis)
+    tiles = jnp.stack(jnp.split(x, peers, axis=split), axis=0)
+    tiles = lax.all_to_all(tiles, axis, split_axis=0, concat_axis=0)
+    return jnp.concatenate(tiles, axis=join)
 
 
 def activate(gate_pre, up_pre):
@@ -76,7 +83,7 @@
     flat_heads = attended.reshape(head_count * head_dim, seq_count, seg_len)
     return jnp.einsum(
         "csr,cm->srm",
-        lax.all_to_all(flat_heads, "tp", split_axis=2, concat_axis=0, tiled=True),
+        trade_parts(flat_heads, "tp", 2, 0),
         mixer_weight,
         preferred_element_type=jnp.float32,
     ).astype(jnp.bfloat16)

time: 131 us -> 136 us (1.038)
  local copies, waits for them, and re-layouts: 14.2 us -> 19.1 us
    unnamed x16 -> x23, local copies, waits for them, and re-layouts: 2.38 us -> 6.61 us
  transfers between devices with their start and end apart: 3 -> 3, of which waited for: 3 -> 2; matrix products, arithmetic and copies ran while one was open for 8% -> 11% of each run, Pallas kernels for 0% -> 0%
where the time goes in v1:
time: 136 us; the launch traced here: 135 us
  blocking collectives  48.1 us (35%)
  starting transfers between devices  23.7 us (17%)
  local copies, waits for them, and re-layouts  19.1 us (14%)
  between operations  14.3 us (11%)
  matrix products  13.2 us (10%)
  other arithmetic  9.63 us (7%)
  waiting for transfers between devices  7.06 us (5%)
    all_to_all x1, blocking collectives, expert_block(): lax.all_to_all(send_rows, 'ep', split_axis=0, concat_axis=0, tiled=True)  30.6 us
    all_to_all x1, starting transfers between devices, expert_block(): lax.all_to_all(summed.astype(jnp.bfloat16), 'ep', split_axis=1, concat_ax...  18.8 us
    all_gather x1, blocking collectives, attend(): value_piece = lax.all_gather(value_vectors, 'ep', axis=3, tiled=True)  8.9 us
    all_gather x1, blocking collectives, attend(): key_piece = lax.all_gather(key_vectors, 'ep', axis=3, tiled=True)  8.59 us
    dot_general x1, matrix products, expert_block(): jnp.einsum('sjcf,jfd->dsjc', hidden, down_part, preferred_element_type=jn...  7.28 us
    unnamed x23, local copies, waits for them, and re-layouts  6.61 us
    all_to_all x1, waiting for transfers between devices, trade_parts(): tiles = lax.all_to_all(tiles, axis, split_axis=0, concat_axis=0)  5.35 us
    all_to_all x1, starting transfers between devices, trade_parts(): tiles = lax.all_to_all(tiles, axis, split_axis=0, concat_axis=0)  4.87 us
  transfers between devices with their start and end apart: 3, of which 2 were waited for; matrix products, arithmetic and copies ran while one was open for 11% of the time, Pallas kernels for 0%

profile of v1, /device:TPU:0, one launch (start us, length us, event | category | flops | bytes accessed | tf_op | source)
XLA Modules:
  0.0 135.3 jit_solution(4806089767754870516)
XLA Ops:
  7.2 0.8 copy.75
  10.2 1.4 %scatter_custom_fusion.1 = s32[512]{0:T(512)S(1)} fusion(s32[256]{0:T(256)S(1)} %bitcast.108, s32[256]{0:T(256)S(1)} %and_select_fusion, s32[]{:T(128)} %copy.136), kind=kCustom, calls=%fused_computation.97 | custom fusion | bytes 2052 | tf_op jit(solution)/shard_map/scatter | solution.py:139
  11.6 1.2 fusion.73
  12.8 1.4 %scatter_custom_fusion = s32[512]{0:T(512)S(1)} fusion(s32[256]{0:T(256)S(1)} %bitcast.109, s32[256]{0:T(256)S(1)} %broadcast.130, s32[]{:T(128)} %copy.136), kind=kCustom, calls=%fused_computation.100 | custom fusion | bytes 2052 | tf_op jit(solution)/shard_map/scatter | solution.py:140
  14.3 1.2 fusion.75
  15.6 2.5 %gather_fusion = bf16[512,2048]{1,0:T(8,128)(2,1)S(1)} fusion(bf16[128,2048]{1,0:T(8,128)(2,1)S(1)} %fusion.75, s32[1024]{0:T(1024)S(1)} %pad_clamp_fusion.1), kind=kCustom, calls=%fused_computation | custom fusion | bytes 4196352 | tf_op jit(solution)/shard_map/gather | solution.py:141
  18.3 30.6 %all_to_all.19 = bf16[8,64,2048]{2,1,0:T(8,128)(2,1)S(1)} all-to-all(bf16[8,64,2048]{2,1,0:T(8,128)(2,1)S(1)} %broadcast_select_fusion), channel_id=1, replica_groups=mesh['ep'=4,'tp'=8] {'ep'}, dimensions={0} | all-to-all | bytes 4194304 | tf_op jit(solution)/shard_map/all_to_all | solution.py:97
  48.9 1.3 fusion.57
  50.2 7.3 %fusion.29 = bf16[2048,4,2,64]{0,3,1,2:T(8,128)(2,1)} fusion(bf16[2,512,2048]{2,1,0:T(8,128)(2,1)} %param.25, f32[2,4,64,512]{3,2,1,0:T(8,128)S(1)} %fusion.57, bf16[2,2048,512]{2,1,0:T(8,128)(2,1)} %param.24, bf16[4,2,64,2048]{3,2,1,0:T(8,128)(2,1)S(1)} %bitcast.103), kind=kOutput, calls=%fused_computation.36 | convolution fusion | flops 2150891520 | bytes 13631488 | tf_op jit(solution)/shard_map/sjcf,jfd->dsjc/dot_general | solution.py:105
  57.5 3.2 %copy.82 = bf16[2048,4,2,64]{0,3,2,1:T(8,128)(2,1)} copy(bf16[2048,4,2,64]{0,3,1,2:T(8,128)(2,1)} %fusion.29) | data formatting | bytes 4194304 | tf_op jit(solution)/shard_map/convert_element_type | solution.py:109
  60.7 0.8 copy-done
  61.6 8.6 %all_gather.6 = bf16[2,64,2,512]{3,1,2,0:T(8,128)(2,1)S(1)} all-gather(bf16[2,64,2,128]{3,1,2,0:T(8,128)(2,1)S(1)} %copy.62), channel_id=1, replica_groups=mesh['ep'=4,'tp'=8] {'ep'}, dimensions={3}, use_global_device_ids=true | all-gather | bytes 327680 | tf_op jit(solution)/shard_map/all_gather | solution.py:53
  70.2 8.9 %all_gather.7 = bf16[2,64,2,512]{3,1,2,0:T(8,128)(2,1)S(1)} all-gather(bf16[2,64,2,128]{3,1,2,0:T(8,128)(2,1)S(1)} %copy.63), channel_id=1, replica_groups=mesh['ep'=4,'tp'=8] {'ep'}, dimensions={3}, use_global_device_ids=true | all-gather | bytes 327680 | tf_op jit(solution)/shard_map/all_gather | solution.py:54
  79.1 5.7 %while.15 = (s32[]{:T(128)}, f32[4,2,64,2,128]{4,2,3,1,0:T(8,128)S(1)}, f32[4,2,2,128]{3,2,1,0:T(2,128)S(1)}, s32[]{:T(128)}, bf16[2,64,2,512]{3,1,2,0:T(8,128)(...) while((s32[]{:T(128)}, ...), condition=%wide.region_5.6_spmd, body=%wide.region_0.5_spmd.sunk | while | flops 27098632 | bytes 2218215 | solution.py:76
  79.1 5.4 %conditional.2 = (f32[1,2,64,2,128]{4,2,3,1,0:T(8,128)S(1)}, f32[1,2,2,128]{3,2,1,0:T(2,128)S(1)}) conditional(s32[]{:T(128)} %convert_element_type.99, () %tuple.72, (s32[]{:T(128)}, s32[]{:T(128)}, bf16[2,64,2,512]{3,1,2,0:T(8,128)(2,1)S(1)}, bf16[2,64,2,128]{3,1,2,0:T(8,128)(2,1)S(1)}, bf16[2,64,2,512]{3,1,2,0:T(8,128)(2,1)S(1)}) %tuple.73), branch_computations={%region_1.0_spmd, %region_2.4_spmd} | conditional | flops 27098628 | bytes 1951828 | solution.py:71
  79.5 4.4 %reduce_window_sum.35 = f32[2,2,128,128]{2,3,1,0:T(8,128)S(1)} reduce-window(f32[2,2,128,128]{2,3,1,0:T(8,128)S(1)} %get-tuple-element.270, f32[]{:T(128)} %constant.130.clone), window={size=1x1x1x128 pad=0_0x0_0x0_0x0_127}, to_apply=%region_3.2 | reduce-window | flops 8323072 | bytes 524292 | tf_op jit(solution)/shard_map/while/body/eval_jaxpr/cond/branch_1_fun/reduce_window_sum | solution.py:37
  90.7 4.9 %all-to-all-start = ((bf16[8,128,2,16]{1,3,2,0:T(8,128)(2,1)}), bf16[8,128,2,16]{1,3,2,0:T(8,128)(2,1)S(1)}, u32[]{:S(2)}, u32[]{:S(2)}) async-start(bf16[8,128,2,16]{1,3,2,0:T(8,128)(2,1)} %constant_dynamic-update-slice_fusion.2), calls=%async_computation | async-start | bytes 131072 | tf_op jit(solution)/shard_map/all_to_all | solution.py:14
  96.1 5.4 %all-to-all-done = bf16[8,128,2,16]{1,3,2,0:T(8,128)(2,1)S(1)} async-done(((bf16[8,128,2,16]{1,3,2,0:T(8,128)(2,1)}), bf16[8,128,2,16]{1,3,2,0:T(8,128)(2,1)S(1)}, u32[]{:S(2)}, u32[]{:S(2)}) %all-to-all-start) | async-done | bytes 65568 | tf_op jit(solution)/shard_map/all_to_all | solution.py:14
  101.5 18.8 %all-to-all-start.2 = ((bf16[256,4,128]{0,2,1:T(8,128)(2,1)}), bf16[256,4,128]{0,2,1:T(8,128)(2,1)S(1)}, u32[]{:S(2)}, u32[]{:S(2)}) async-start(bf16[256,4,128]{0,2,1:T(8,128)(2,1)} %bitcast.105), calls=%async_computation.3 | async-start | bytes 524288 | tf_op jit(solution)/shard_map/all_to_all | solution.py:114
  120.2 3.7 %fusion.32 = bf16[2,16,2048]{2,1,0:T(8,128)(2,1)} fusion(bf16[1024,2048]{1,0:T(8,128)(2,1)} %param.18, bf16[8,128,2,16]{1,3,2,0:T(8,128)(2,1)S(1)} %all-to-all-done), kind=kOutput, calls=%fused_computation.37 | convolution fusion | flops 134283264 | bytes 4390912 | tf_op jit(solution)/shard_map/csr,cm->srm/dot_general | solution.py:84
  123.9 1.7 %all-to-all-done.2 = bf16[256,4,128]{0,2,1:T(8,128)(2,1)S(1)} async-done(((bf16[256,4,128]{0,2,1:T(8,128)(2,1)}), bf16[256,4,128]{0,2,1:T(8,128)(2,1)S(1)}, u32[]{:S(2)}, u32[]{:S(2)}) %all-to-all-start.2) | async-done | bytes 262176 | tf_op jit(solution)/shard_map/all_to_all | solution.py:114
  125.7 1.0 gather_fusion.1
  126.8 0.9 multiply_reduce_fusion.1
  127.7 0.7 copy.84
  (90 shorter events, 10.3 us)
Async XLA Ops:
  7.2 94.3 %reduce-scatter.2.cloned.1.call-start = ((), (), s32[]{:S(2)}) async-start(), calls=%async_computation.4 | async-start | bytes 2359296 | tf_op jit(solution)/shard_map/reduce_scatter | solution.py:106
  18.3 30.6 %copy-start.5 = (bf16[2,2048,512]{2,1,0:T(8,128)(2,1)S(1)}, bf16[2,2048,512]{2,1,0:T(8,128)(2,1)}, u32[]{:S(2)}) copy-start(bf16[2,2048,512]{2,1,0:T(8,128)(2,1)} %param.23) | copy-start | bytes 12582916
  60.7 0.8 copy-start
  60.7 0.9 copy-start.1
  60.7 0.9 copy-start.2
  84.8 10.9 %copy-start.4 = (f32[128,2]{0,1:T(2,128)S(1)}, f32[128,2]{0,1:T(2,128)}, u32[]{:S(2)}) copy-start(f32[128,2]{0,1:T(2,128)} %param.22) | copy-start | bytes 3076
  84.9 11.0 %copy-start.3 = (s32[128,2]{0,1:T(2,128)S(1)}, s32[128,2]{0,1:T(2,128)}, u32[]{:S(2)}) copy-start(s32[128,2]{0,1:T(2,128)} %param.21) | copy-start | bytes 3076
  90.7 10.8 %all-to-all-start = ((bf16[8,128,2,16]{1,3,2,0:T(8,128)(2,1)}), bf16[8,128,2,16]{1,3,2,0:T(8,128)(2,1)S(1)}, u32[]{:S(2)}, u32[]{:S(2)}) async-start(bf16[8,128,2,16]{1,3,2,0:T(8,128)(2,1)} %constant_dynamic-update-slice_fusion.2), calls=%async_computation | async-start | bytes 131072 | tf_op jit(solution)/shard_map/all_to_all | solution.py:14
  101.5 24.1 %all-to-all-start.2 = ((bf16[256,4,128]{0,2,1:T(8,128)(2,1)}), bf16[256,4,128]{0,2,1:T(8,128)(2,1)S(1)}, u32[]{:S(2)}, u32[]{:S(2)}) async-start(bf16[256,4,128]{0,2,1:T(8,128)(2,1)} %bitcast.105), calls=%async_computation.3 | async-start | bytes 524288 | tf_op jit(solution)/shard_map/all_to_all | solution.py:114
Sparse Core Ops, SparseCore 0:
  60.8 35.5 reduce-scatter.1
